TPU v7x, 32 devices: a whole 2x2x4 slice. The times are simulated.
32 devices in a mesh: dp: 4 (over y, x), kv: 4 (over z), tp: 2 (over core).
Axes of the slice: x: 2, y: 2, z: 4, core: 2. Of those that a mesh axis runs over, the one named last changes fastest.
Arguments:
- tokens: bfloat16 [4, 1536, 2048], P('dp', 'kv'), may hold values from -21 to 21
- seq_lengths: int32 [4], P('dp'), may hold values from 1 to 1536, 2304 in all
- block_picks: int32 [4, 24, 4, 16], P('dp', 'kv', 'tp'), may hold values from -1 to 17, as said below
- w_query: bfloat16 [2048, 1024], P('kv', 'tp'), may hold values from -0.125 to 0.125
- w_key: bfloat16 [2048, 256], P('kv', 'tp'), may hold values from -0.125 to 0.125
- w_value: bfloat16 [2048, 256], P('kv', 'tp'), may hold values from -0.125 to 0.125
- w_gate: bfloat16 [2048, 32], replicated, may hold values from -0.125 to 0.125
- w_ckey: bfloat16 [4096, 64], replicated, may hold values from -0.09375 to 0.09375
- w_cvalue: bfloat16 [4096, 64], replicated, may hold values from -0.09375 to 0.09375
- w_out: bfloat16 [1024, 2048], P('tp', 'kv'), may hold values from -0.1875 to 0.1875
Outputs:
- attention_out: bfloat16 [4, 1536, 2048], P('dp', ('kv', 'tp'))
Inputs may be any that keep to these rules, and one draw needn't show every extreme that they name: `block_picks`: A query block's entries name distinct blocks that all lie in earlier spans of 384 positions, or are -1; the largest such block is named in every draw. For one span and one group, the entries of all its query blocks together name blocks of any one other span at most 2 times; this is reached in every draw.
All inputs are finite; a program needn't handle non-finite values. No bound on the sum of `seq_lengths` on one device may be relied on, other than what follows from the above.
Results may differ from a plain program's by a relative error of at most 0.01.
The roundings to bfloat16 on the way count: a program that leaves them out, or rounds other values in their place, can miss the bound.
Values may be sent and summed in bfloat16 or wider, within the bound.
No kernel may reach another device: no remote copies, remote signals or barrier semaphores. Data moves between devices by JAX's collectives and lax.ppermute only.
A program may use at most 64 MiB of HBM per device.

v0:
```python
import jax
import jax.numpy as jnp
from jax import lax
from jax.sharding import PartitionSpec as P

HEADS = 16
HEAD = 64
BLK = 64
PICKS = 16


masked_low = -1e30


def body(
    tokens, seq_lengths, block_picks, w_query, w_key, w_value, w_gate, w_ckey, w_cvalue, w_out
):
    token_rows = tokens[0]
    tok_count = token_rows.shape[0]
    shard_index = lax.axis_index("kv")
    head_index = lax.axis_index("tp")
    group_count = w_key.shape[1] // HEAD
    head_count = w_query.shape[1] // HEAD
    per_group = head_count // group_count
    block_count = tok_count // BLK
    inv_scale = HEAD ** (-0.5)
    zero_query = jnp.zeros((tok_count, w_query.shape[1]), jnp.float32)
    zero_key = jnp.zeros((tok_count, w_key.shape[1]), jnp.float32)
    runnings = (zero_query, zero_key, zero_key)
    weight_pieces = (
        lax.all_gather(w_query, "kv", axis=0, tiled=True),
        lax.all_gather(w_key, "kv", axis=0, tiled=True),
        lax.all_gather(w_value, "kv", axis=0, tiled=True),
    )
    collected = []
    for running, weight_piece in zip(runnings, weight_pieces):
        collected.append(jnp.dot(token_rows, weight_piece, preferred_element_type=jnp.float32))
    query_sum, key_sum, value_sum = tuple(collected)
    queries = query_sum.astype(jnp.bfloat16).reshape(block_count, BLK, group_count, per_group, HEAD)
    key_blocks = (
        key_sum.astype(jnp.bfloat16)
        .reshape(block_count, BLK, group_count, HEAD)
        .transpose(0, 2, 1, 3)
    )
    value_blocks = (
        value_sum.astype(jnp.bfloat16)
        .reshape(block_count, BLK, group_count, HEAD)
        .transpose(0, 2, 1, 3)
    )
    gate_all = jax.nn.sigmoid(jnp.dot(token_rows, w_gate, preferred_element_type=jnp.float32))
    gate_local = lax.dynamic_slice_in_dim(
        gate_all.reshape(tok_count, 2, HEADS), head_index * head_count, head_count, 2
    )
    gate_local = gate_local.reshape(block_count, BLK, 2, group_count, per_group)
    ckeys = jnp.dot(
        key_blocks.reshape(block_count * group_count, BLK * HEAD),
        w_ckey,
        preferred_element_type=jnp.float32,
    ).astype(jnp.bfloat16)
    cvalues = jnp.dot(
        value_blocks.reshape(block_count * group_count, BLK * HEAD),
        w_cvalue,
        preferred_element_type=jnp.float32,
    ).astype(jnp.bfloat16)
    cpairs = jnp.concatenate([ckeys, cvalues], axis=-1).reshape(block_count, group_count, 2 * HEAD)
    pair_blocks = jnp.concatenate([key_blocks, value_blocks], axis=-1)
    chosen = block_picks[0]
    usable = chosen >= 0
    group_ids = jnp.arange(group_count, dtype=jnp.int32)
    every_pair, every_cpair = (
        lax.all_gather(pair_blocks, "kv", axis=0, tiled=True),
        lax.all_gather(cpairs, "kv", axis=0, tiled=True),
    )
    flat_pairs = every_pair.reshape(-1, BLK, 2 * HEAD)
    lookup = jnp.where(usable, chosen, 0) * group_count + group_ids[None, :, None]
    fetched = flat_pairs[lookup]
    comp_keys = every_cpair[..., :HEAD]
    comp_values = every_cpair[..., HEAD:]
    block_ends = jnp.arange(every_cpair.shape[0], dtype=jnp.int32) * BLK + (BLK - 1)
    causal = jnp.arange(BLK)[None, :] <= jnp.arange(BLK)[:, None]

    def attend(block_inputs):
        qblock, gblock, own_pair, far_pair, far_usable, block_index = block_inputs
        query_spots = shard_index * tok_count + block_index * BLK + jnp.arange(BLK, dtype=jnp.int32)
        comp_score = (
            jnp.einsum("tgpd,cgd->gtpc", qblock, comp_keys, preferred_element_type=jnp.float32)
            * inv_scale
        )
        visible = (block_ends[None, :] <= query_spots[:, None])[None, :, None, :]
        comp_score = jnp.where(visible, comp_score, masked_low)
        comp_top = jnp.max(comp_score, axis=-1, keepdims=True)
        comp_weight = jnp.where(visible, jnp.exp(comp_score - comp_top), 0.0)
        comp_sum = jnp.maximum(jnp.sum(comp_weight, axis=-1, keepdims=True), 1.0)
        comp_prob = (comp_weight / comp_sum).astype(jnp.bfloat16)
        comp_out = jnp.einsum(
            "gtpc,cgd->tgpd", comp_prob, comp_values, preferred_element_type=jnp.float32
        )
        far_pairs = far_pair.reshape(group_count, PICKS * BLK, 2 * HEAD)
        own_score = (
            jnp.einsum(
                "tgpd,gsd->gtps", qblock, own_pair[..., :HEAD], preferred_element_type=jnp.float32
            )
            * inv_scale
        )
        own_mask = causal[None, :, None, :]
        own_score = jnp.where(own_mask, own_score, masked_low)
        far_score = (
            jnp.einsum(
                "tgpd,gkd->gtpk", qblock, far_pairs[..., :HEAD], preferred_element_type=jnp.float32
            )
            * inv_scale
        )
        far_mask = jnp.repeat(far_usable, BLK, axis=-1)[:, None, None, :]
        far_score = jnp.where(far_mask, far_score, masked_low)
        score_top = jnp.maximum(
            jnp.max(own_score, axis=-1, keepdims=True), jnp.max(far_score, axis=-1, keepdims=True)
        )
        own_weight = jnp.where(own_mask, jnp.exp(own_score - score_top), 0.0)
        far_weight = jnp.where(far_mask, jnp.exp(far_score - score_top), 0.0)
        normalizer = jnp.sum(own_weight, axis=-1, keepdims=True) + jnp.sum(
            far_weight, axis=-1, keepdims=True
        )
        own_prob = (own_weight / normalizer).astype(jnp.bfloat16)
        far_prob = (far_weight / normalizer).astype(jnp.bfloat16)
        chosen_out = jnp.einsum(
            "gtps,gsd->tgpd", own_prob, own_pair[..., HEAD:], preferred_element_type=jnp.float32
        ) + jnp.einsum(
            "gtpk,gkd->tgpd", far_prob, far_pairs[..., HEAD:], preferred_element_type=jnp.float32
        )
        mixed_out = gblock[:, 0, :, :, None] * comp_out + gblock[:, 1, :, :, None] * chosen_out
        return mixed_out.astype(jnp.bfloat16)

    attended = lax.map(
        attend,
        (
            queries,
            gate_local,
            pair_blocks,
            fetched,
            usable,
            jnp.arange(block_count, dtype=jnp.int32),
        ),
    )
    attended = attended.reshape(tok_count, head_count * HEAD)
    out_full = lax.all_gather(w_out, "kv", axis=1, tiled=True)
    half_rows = tok_count // lax.axis_size("tp")
    summed = lax.psum_scatter(
        jnp.dot(attended, out_full, preferred_element_type=jnp.float32).astype(jnp.bfloat16),
        "tp",
        scatter_dimension=0,
        tiled=True,
    ).astype(jnp.float32)
    out_positions = (
        shard_index * tok_count + head_index * half_rows + jnp.arange(half_rows, dtype=jnp.int32)
    )
    live_rows = out_positions < seq_lengths[0]
    return jnp.where(live_rows[:, None], summed, 0.0).astype(jnp.bfloat16)[None]


def solution(mesh):
    return jax.shard_map(
        body,
        mesh=mesh,
        in_specs=(
            P("dp", "kv", None),
            P("dp"),
            P("dp", "kv", "tp", None),
            P("kv", "tp"),
            P("kv", "tp"),
            P("kv", "tp"),
            P(),
            P(),
            P(),
            P("tp", "kv"),
        ),
        out_specs=P("dp", ("kv", "tp"), None),
        check_vma=False,
    )
```

profile of v0, /device:TPU:0, one launch (start us, length us, event | category | flops | bytes accessed | tf_op | source)
XLA Modules:
  0.0 189.2 jit_solution(17101830072245210733)
XLA Ops:
  8.1 20.5 %all_gather.19 = bf16[2048,128]{1,0:T(8,128)(2,1)S(1)} all-gather(bf16[512,128]{1,0:T(8,128)(2,1)} %param.16), channel_id=1, replica_groups=mesh['dp'=4,'kv'=4,'tp'=2] {'kv'}, dimensions={0}, use_global_device_ids=true | all-gather | bytes 655360 | tf_op jit(solution)/shard_map/all_gather | solution.py:32
  29.3 22.5 %all_gather.20 = bf16[2048,128]{1,0:T(8,128)(2,1)S(1)} all-gather(bf16[512,128]{1,0:T(8,128)(2,1)S(1)} %copy-done.3), channel_id=1, replica_groups=mesh['dp'=4,'kv'=4,'tp'=2] {'kv'}, dimensions={0}, use_global_device_ids=true | all-gather | bytes 655360 | tf_op jit(solution)/shard_map/all_gather | solution.py:33
  53.9 26.7 %all_gather.22 = bf16[24,2,64,128]{3,2,1,0:T(8,128)(2,1)S(1)} all-gather(bf16[6,2,64,128]{3,2,1,0:T(8,128)(2,1)S(1)} %pad_maximum_fusion), channel_id=1, replica_groups=mesh['dp'=4,'kv'=4,'tp'=2] {'kv'}, dimensions={0}, use_global_device_ids=true | all-gather | bytes 983040 | tf_op jit(solution)/shard_map/all_gather | solution.py:71
  80.9 1.3 convolution_convert_fusion.2
  82.3 13.5 %all_gather.21 = bf16[24,2,128]{2,1,0:T(2,128)(2,1)S(1)} all-gather(bf16[6,2,128]{2,1,0:T(2,128)(2,1)S(1)} %reshape.147), channel_id=1, replica_groups=mesh['dp'=4,'kv'=4,'tp'=2] {'kv'}, dimensions={0}, use_global_device_ids=true | all-gather | bytes 15360 | tf_op jit(solution)/shard_map/all_gather | solution.py:72
  95.9 2.7 %gather_fusion = bf16[192,64,128]{2,1,0:T(8,128)(2,1)} fusion(bf16[48,64,128]{2,1,0:T(8,128)(2,1)S(1)} %bitcast.174, s32[1024]{0:T(1024)S(1)} %pad_clamp_fusion), kind=kCustom, calls=%fused_computation | custom fusion | bytes 6292224 | tf_op jit(solution)/shard_map/gather | solution.py:76
  98.7 2.6 %fusion.40 = bf16[384,512]{1,0:T(8,128)(2,1)S(1)} fusion(bf16[2048,512]{1,0:T(8,128)(2,1)} %all-gather.3.cloned.1.call-done, bf16[1,384,2048]{2,1,0:T(8,128)(2,1)S(1)} %copy-done), kind=kOutput, calls=%fused_computation.69 | convolution fusion | flops 805502976 | bytes 4063232 | tf_op jit(solution)/shard_map/dot_general | solution.py:37
  101.7 65.3 %while.14 = (s32[]{:T(128)}, bf16[6,64,2,4,64]{4,3,2,1,0:T(4,128)(2,1)}, f32[6,64,2,2,4]{1,0,4,3,2:T(8,128)S(1)}, s32[6]{0:T(128)S(1)}, s32[]{:T(128)}, /*index=...) while((s32[]{:T(128)}, ...), condition=%wide.region_7.8_spmd.clone.clone, body=%wide.region_0.7_spmd.clone.clone.sunk | while | flops 153700000 | bytes 18673140 | solution.py:133
  101.9 1.1 constant_dynamic-slice_fusion.9
  103.9 1.0 copy-done.1
  105.6 1.0 fusion.103
  108.3 0.9 fusion.98
  109.3 2.5 %fusion.104 = bf16[1,64,2,4,64]{4,1,3,2,0:T(8,128)(2,1)S(1)} fusion(f32[64,2,4,64]{3,0,2,1:T(8,128)} %fusion.98, f32[2,64,64,4]{1,2,3,0:T(8,128)} %fusion.103, f32[2,64,4,1024]{3,1,2,0:T(8,128)} %copy-done.1, f32[2,64,4]{1,2,0:T(4,128)S(1)} %add.172, f32[2,64,4]{1,2,0:T(4,128)S(1)} %max.28, pred[2,1024]{1,0:T(4,128)(4,1)S(1)} %broadcast_in_dim.226, ...), kind=kOutput, calls=%fused_computation.19.clone.1 | convolution fusion | flops 70385664 | bytes 2957312 | tf_op jit(solution)/shard_map/while/body/eval_jaxpr/gtpk,gkd->tgpd/dot_general | solution.py:127
  111.8 0.8 copy_dynamic-update-slice_fusion.2
  112.8 1.1 constant_dynamic-slice_fusion.9
  114.8 1.0 copy-done.1
  116.5 1.0 fusion.103
  119.3 0.9 fusion.98
  120.2 2.5 %fusion.104 = bf16[1,64,2,4,64]{4,1,3,2,0:T(8,128)(2,1)S(1)} fusion(f32[64,2,4,64]{3,0,2,1:T(8,128)} %fusion.98, f32[2,64,64,4]{1,2,3,0:T(8,128)} %fusion.103, f32[2,64,4,1024]{3,1,2,0:T(8,128)} %copy-done.1, f32[2,64,4]{1,2,0:T(4,128)S(1)} %add.172, f32[2,64,4]{1,2,0:T(4,128)S(1)} %max.28, pred[2,1024]{1,0:T(4,128)(4,1)S(1)} %broadcast_in_dim.226, ...), kind=kOutput, calls=%fused_computation.19.clone.1 | convolution fusion | flops 70385664 | bytes 2957312 | tf_op jit(solution)/shard_map/while/body/eval_jaxpr/gtpk,gkd->tgpd/dot_general | solution.py:127
  122.7 0.8 copy_dynamic-update-slice_fusion.2
  123.7 1.1 constant_dynamic-slice_fusion.9
  125.6 1.0 copy-done.1
  127.4 1.0 fusion.103
  130.1 0.9 fusion.98
  131.1 2.5 %fusion.104 = bf16[1,64,2,4,64]{4,1,3,2,0:T(8,128)(2,1)S(1)} fusion(f32[64,2,4,64]{3,0,2,1:T(8,128)} %fusion.98, f32[2,64,64,4]{1,2,3,0:T(8,128)} %fusion.103, f32[2,64,4,1024]{3,1,2,0:T(8,128)} %copy-done.1, f32[2,64,4]{1,2,0:T(4,128)S(1)} %add.172, f32[2,64,4]{1,2,0:T(4,128)S(1)} %max.28, pred[2,1024]{1,0:T(4,128)(4,1)S(1)} %broadcast_in_dim.226, ...), kind=kOutput, calls=%fused_computation.19.clone.1 | convolution fusion | flops 70385664 | bytes 2957312 | tf_op jit(solution)/shard_map/while/body/eval_jaxpr/gtpk,gkd->tgpd/dot_general | solution.py:127
  133.6 0.8 copy_dynamic-update-slice_fusion.2
  134.6 1.1 constant_dynamic-slice_fusion.9
  136.5 1.0 copy-done.1
  138.3 1.0 fusion.103
  141.0 0.9 fusion.98
  142.0 2.5 %fusion.104 = bf16[1,64,2,4,64]{4,1,3,2,0:T(8,128)(2,1)S(1)} fusion(f32[64,2,4,64]{3,0,2,1:T(8,128)} %fusion.98, f32[2,64,64,4]{1,2,3,0:T(8,128)} %fusion.103, f32[2,64,4,1024]{3,1,2,0:T(8,128)} %copy-done.1, f32[2,64,4]{1,2,0:T(4,128)S(1)} %add.172, f32[2,64,4]{1,2,0:T(4,128)S(1)} %max.28, pred[2,1024]{1,0:T(4,128)(4,1)S(1)} %broadcast_in_dim.226, ...), kind=kOutput, calls=%fused_computation.19.clone.1 | convolution fusion | flops 70385664 | bytes 2957312 | tf_op jit(solution)/shard_map/while/body/eval_jaxpr/gtpk,gkd->tgpd/dot_general | solution.py:127
  144.5 0.8 copy_dynamic-update-slice_fusion.2
  145.5 1.1 constant_dynamic-slice_fusion.9
  147.4 1.0 copy-done.1
  149.2 1.0 fusion.103
  151.9 0.9 fusion.98
  152.8 2.5 %fusion.104 = bf16[1,64,2,4,64]{4,1,3,2,0:T(8,128)(2,1)S(1)} fusion(f32[64,2,4,64]{3,0,2,1:T(8,128)} %fusion.98, f32[2,64,64,4]{1,2,3,0:T(8,128)} %fusion.103, f32[2,64,4,1024]{3,1,2,0:T(8,128)} %copy-done.1, f32[2,64,4]{1,2,0:T(4,128)S(1)} %add.172, f32[2,64,4]{1,2,0:T(4,128)S(1)} %max.28, pred[2,1024]{1,0:T(4,128)(4,1)S(1)} %broadcast_in_dim.226, ...), kind=kOutput, calls=%fused_computation.19.clone.1 | convolution fusion | flops 70385664 | bytes 2957312 | tf_op jit(solution)/shard_map/while/body/eval_jaxpr/gtpk,gkd->tgpd/dot_general | solution.py:127
  155.4 0.8 copy_dynamic-update-slice_fusion.2
  156.4 1.1 constant_dynamic-slice_fusion.9
  158.3 1.0 copy-done.1
  160.1 1.0 fusion.103
  162.8 0.9 fusion.98
  163.7 2.5 %fusion.104 = bf16[1,64,2,4,64]{4,1,3,2,0:T(8,128)(2,1)S(1)} fusion(f32[64,2,4,64]{3,0,2,1:T(8,128)} %fusion.98, f32[2,64,64,4]{1,2,3,0:T(8,128)} %fusion.103, f32[2,64,4,1024]{3,1,2,0:T(8,128)} %copy-done.1, f32[2,64,4]{1,2,0:T(4,128)S(1)} %add.172, f32[2,64,4]{1,2,0:T(4,128)S(1)} %max.28, pred[2,1024]{1,0:T(4,128)(4,1)S(1)} %broadcast_in_dim.226, ...), kind=kOutput, calls=%fused_computation.19.clone.1 | convolution fusion | flops 70385664 | bytes 2957312 | tf_op jit(solution)/shard_map/while/body/eval_jaxpr/gtpk,gkd->tgpd/dot_general | solution.py:127
  166.2 0.8 copy_dynamic-update-slice_fusion.2
  167.0 2.0 %reshape.149 = bf16[384,512]{1,0:T(8,128)(2,1)S(1)} reshape(bf16[6,64,2,4,64]{4,3,2,1,0:T(4,128)(2,1)} %get-tuple-element.157) | data formatting | bytes 786432 | tf_op jit(solution)/shard_map/reshape | solution.py:144
  169.1 3.7 %convolution_convert_fusion = bf16[384,2048]{1,0:T(8,128)(2,1)} fusion(bf16[384,512]{1,0:T(8,128)(2,1)S(1)} %reshape.149, bf16[512,2048]{1,0:T(8,128)(2,1)} %all-gather.5.cloned.1.call-done), kind=kOutput, calls=%fused_computation.59 | convolution fusion | flops 806092800 | bytes 4063232 | tf_op jit(solution)/shard_map/dot_general | solution.py:148
  173.5 6.9 %reduce-scatter.2.cloned.1.call-done = bf16[192,2048]{1,0:T(8,128)(2,1)} async-done(((bf16[384,2048]{1,0:T(8,128)(2,1)}), bf16[192,2048]{1,0:T(8,128)(2,1)}) %reduce-scatter.2.cloned.1.call-update) | async-done | bytes 786448 | tf_op jit(solution)/shard_map/reduce_scatter | solution.py:147
  180.4 2.2 %fusion.61 = bf16[1,192,2048]{2,1,0:T(8,128)(2,1)} fusion(bf16[192,2048]{1,0:T(8,128)(2,1)} %reduce-scatter.2.cloned.1.call-done, pred[192]{0:T(512)(128)(4,1)S(1)} %add_compare_fusion), kind=kLoop, calls=%fused_computation.78 | loop fusion | flops 1179648 | bytes 1573056 | tf_op jit(solution)/shard_map/broadcast_in_dim | solution.py:157
  (175 shorter events, 21.8 us)
Async XLA Ops:
  6.5 22.0 %copy-start = (bf16[1,384,2048]{2,1,0:T(8,128)(2,1)S(1)}, bf16[1,384,2048]{2,1,0:T(8,128)(2,1)}, u32[]{:S(2)}) copy-start(bf16[1,384,2048]{2,1,0:T(8,128)(2,1)} %param.12) | copy-start | bytes 4718596
  6.5 22.7 %copy-start.3 = (bf16[512,128]{1,0:T(8,128)(2,1)S(1)}, bf16[512,128]{1,0:T(8,128)(2,1)}, u32[]{:S(2)}) copy-start(bf16[512,128]{1,0:T(8,128)(2,1)} %param.17) | copy-start | bytes 393220
  6.5 92.1 %all-gather.3.cloned.1.call-start = ((), (), s32[]{:S(2)}) async-start(), calls=%async_computation.1 | async-start | bytes 2621440 | tf_op jit(solution)/shard_map/all_gather | solution.py:31
  7.3 161.8 %all-gather.5.cloned.1.call-start = ((), (), s32[]{:S(2)}) async-start(), calls=%async_computation.2 | async-start | bytes 2621440 | tf_op jit(solution)/shard_map/all_gather | solution.py:145
  8.0 172.4 %reduce-scatter.2.cloned.1.call-start = ((), (), s32[]{:S(2)}) async-start(), calls=%async_computation.3 | async-start | bytes 2359296 | tf_op jit(solution)/shard_map/reduce_scatter | solution.py:147
  51.8 1.3 copy-start.5
  51.8 1.4 copy-start.4
  52.6 28.0 %copy-start.2 = (bf16[4096,64]{0,1:T(8,128)(2,1)S(1)}, bf16[4096,64]{0,1:T(8,128)(2,1)}, u32[]{:S(2)}) copy-start(bf16[4096,64]{0,1:T(8,128)(2,1)} %param.20) | copy-start | bytes 1572868
  103.5 1.4 copy-start.1
  114.4 1.4 copy-start.1
  125.3 1.4 copy-start.1
  136.2 1.4 copy-start.1
  147.1 1.4 copy-start.1
  158.0 1.4 copy-start.1
Sparse Core Ops, SparseCore 0:
  8.9 69.9 all-gather.2
  80.5 44.8 all-gather.4
  173.0 7.4 reduce-scatter.1
where the time goes:
time: 190 us; the launch traced here: 189 us
  blocking collectives  83.2 us (44%)
  matrix products  42 us (22%)
  local copies, waits for them, and re-layouts  28.9 us (15%)
  between operations  14 us (7%)
  waiting for transfers between devices  8.37 us (4%)
  other arithmetic  7.92 us (4%)
  loops' own time  4.76 us (3%)
    all_gather x1, blocking collectives, body(): lax.all_gather(pair_blocks, 'kv', axis=0, tiled=True)  26.7 us
    all_gather x1, blocking collectives, body(): lax.all_gather(w_value, 'kv', axis=0, tiled=True)  22.5 us
    all_gather x1, blocking collectives, body(): lax.all_gather(w_key, 'kv', axis=0, tiled=True)  20.5 us
    dot_general x6, matrix products, attend(): jnp.einsum('gtpk,gkd->tgpd', far_prob, far_pairs[..., HEAD:], preferred_e...  15.1 us
    all_gather x1, blocking collectives, body(): lax.all_gather(cpairs, 'kv', axis=0, tiled=True)  13.5 us
    dynamic_slice x24, local copies, waits for them, and re-layouts, body(): lax.map(attend, (queries, gate_local, pair_blocks, fetched, usable, jnp.a...  10.7 us
    reduce_scatter x1, waiting for transfers between devices, body(): lax.psum_scatter(jnp.dot(attended, out_full, preferred_element_type=jnp.f...  6.93 us
    while x12, local copies, waits for them, and re-layouts  6.29 us
  transfers between devices with their start and end apart: 3, of which 1 were waited for; matrix products, arithmetic and copies ran while one was open for 35% of the time, Pallas kernels for 0%

commit v1 on v0

v1 whole, which is shorter than its diff:
```python
import functools

import jax
import jax.numpy as jnp
from jax import lax
from jax.experimental import pallas as pl
from jax.experimental.pallas import tpu as pltpu
from jax.sharding import PartitionSpec as P

HEADS = 16
HEAD = 64
BLK = 64
PICKS = 16
LANES = 128

masked_low = -1e30


def nt_dot(a, b):
    return lax.dot_general(a, b, (((1,), (1,)), ((), ())), preferred_element_type=jnp.float32)


def group_slabs(slab, odd, low_lanes, high_lanes):
    rolled = jnp.concatenate([slab[:, HEAD:], slab[:, :HEAD]], axis=1)
    low, high = (rolled, slab) if odd else (slab, rolled)
    return jnp.concatenate([low * low_lanes, high * high_lanes], axis=0)


def attend_kernel(
    shape, start_ref, picks_ref, q_ref, gate_ref, pairs_ref, comp_ref, out_ref, spill_ref, list_ref
):
    blocks, groups, per_group, span_rows = shape
    pairs = per_group // 2
    rows = pairs * BLK
    kv_width = groups * HEAD
    comp_count = comp_ref.shape[0]
    inv_scale = HEAD ** (-0.5)
    span = start_ref[0]
    lane_row = lax.broadcasted_iota(jnp.int32, (1, LANES), 1)
    low_lanes = jnp.where(lane_row < HEAD, 1.0, 0.0).astype(jnp.bfloat16)
    high_lanes = jnp.where(lane_row < HEAD, 0.0, 1.0).astype(jnp.bfloat16)
    lane = lax.broadcasted_iota(jnp.int32, (rows, LANES), 1)
    spot = lax.broadcasted_iota(jnp.int32, (rows, LANES), 0) % BLK
    low_half = lane < HEAD
    own_seen = low_half & (lane <= spot)
    high_half = jnp.logical_not(low_half)
    comp_lane = lax.broadcasted_iota(jnp.int32, (rows, comp_count), 1)
    comp_spot = lax.broadcasted_iota(jnp.int32, (rows, comp_count), 0) % BLK

    def block_rows(block):
        at = block // blocks
        row = pl.multiple_of((block - at * blocks) * BLK, BLK)
        return at, pl.ds(row, BLK)

    def two_heads(s, n):
        return s[:, :n], s[:, n:]

    def top(s, mask):
        s = jnp.where(mask, s, masked_low)
        return s, jnp.max(s, axis=1, keepdims=True)

    def key_values(block_a, block_b, g):
        column = (g // 2) * LANES
        parts = []
        for base in (column, kv_width + column):
            a_span, a_rows = block_rows(block_a)
            b_span, b_rows = block_rows(block_b)
            slab = jnp.concatenate(
                [
                    pairs_ref[a_span, a_rows, base : base + LANES],
                    pairs_ref[b_span, b_rows, base : base + LANES],
                ],
                axis=0,
            )
            parts.append(group_slabs(slab, g % 2, low_lanes, high_lanes))
        return parts

    comp_parts = []
    for g in range(groups):
        column = (g // 2) * LANES
        comp_parts.append(
            [
                group_slabs(comp_ref[:, base : base + LANES], g % 2, low_lanes, high_lanes)
                for base in (column, kv_width + column)
            ]
        )

    def one_block(b, _):
        here = pl.ds(pl.multiple_of(b * BLK, BLK), BLK)
        gates = gate_ref[here, :]
        for g in range(groups):
            count = jnp.int32(0)
            for k in range(PICKS):
                pick = picks_ref[b, g * PICKS + k]
                list_ref[count] = pick
                count = count + (pick >= 0).astype(jnp.int32)
            first = jnp.maximum(list_ref[0], 0)
            queries = jnp.concatenate(
                [
                    q_ref[here, (g * pairs + p) * LANES : (g * pairs + p + 1) * LANES]
                    for p in range(pairs)
                ],
                axis=0,
            )
            ckeys, cvalues = comp_parts[g]
            comp_seen = (comp_lane + 1) * BLK - 1 <= (span * blocks + b) * BLK + comp_spot
            comp_probs = []
            for s in two_heads(nt_dot(queries, ckeys) * inv_scale, comp_count):
                s, m = top(s, comp_seen)
                w = jnp.where(comp_seen, jnp.exp(s - m), 0.0)
                total = jnp.maximum(jnp.sum(w, axis=1, keepdims=True), 1.0)
                comp_probs.append((w * (1.0 / total)).astype(jnp.bfloat16))
            comp_out = jnp.dot(
                jnp.concatenate(comp_probs, axis=1), cvalues, preferred_element_type=jnp.float32
            )
            keys, values = key_values(span * blocks + b, first, g)
            seen = own_seen | (high_half & (jnp.full((rows, LANES), count) > 0))
            (s0, m0), (s1, m1) = [
                top(s, seen) for s in two_heads(nt_dot(queries, keys) * inv_scale, LANES)
            ]
            steps = count // 2

            def far_blocks(i):
                second_there = 2 * i + 2 < count
                block_a = list_ref[2 * i + 1]
                block_b = jnp.where(second_there, list_ref[2 * i + 2], block_a)
                return block_a, block_b, second_there

            def scan(i, tops):
                block_a, block_b, second_there = far_blocks(i)
                far_keys, _ = key_values(block_a, block_b, g)
                limit = jnp.where(second_there, LANES, HEAD)
                far_seen = lane < jnp.full((rows, LANES), limit)
                s = two_heads(nt_dot(queries, far_keys) * inv_scale, LANES)
                (a, ma), (c, mc) = [top(x, far_seen) for x in s]
                spill_ref[i, :, :LANES] = a
                spill_ref[i, :, LANES:] = c
                return jnp.maximum(tops[0], ma), jnp.maximum(tops[1], mc)

            m0, m1 = lax.fori_loop(0, steps, scan, (m0, m1))
            w0, w1 = jnp.exp(s0 - m0), jnp.exp(s1 - m1)
            l0 = jnp.sum(w0, axis=1, keepdims=True)
            l1 = jnp.sum(w1, axis=1, keepdims=True)

            def add_up(i, sums):
                a = jnp.exp(spill_ref[i, :, :LANES] - m0)
                c = jnp.exp(spill_ref[i, :, LANES:] - m1)
                spill_ref[i, :, :LANES] = a
                spill_ref[i, :, LANES:] = c
                return (
                    sums[0] + jnp.sum(a, axis=1, keepdims=True),
                    sums[1] + jnp.sum(c, axis=1, keepdims=True),
                )

            l0, l1 = lax.fori_loop(0, steps, add_up, (l0, l1))
            r0, r1 = 1.0 / l0, 1.0 / l1

            def weigh(a, c, far_values):
                probs = jnp.concatenate(
                    [(a * r0).astype(jnp.bfloat16), (c * r1).astype(jnp.bfloat16)], axis=1
                )
                return jnp.dot(probs, far_values, preferred_element_type=jnp.float32)

            def gather(i, total):
                block_a, block_b, _ = far_blocks(i)
                _, far_values = key_values(block_a, block_b, g)
                return total + weigh(spill_ref[i, :, :LANES], spill_ref[i, :, LANES:], far_values)

            chosen_out = lax.fori_loop(0, steps, gather, weigh(w0, w1, values))
            for p in range(pairs):
                h = g * per_group + 2 * p
                part = slice(p * BLK, (p + 1) * BLK)
                low = low_half[part]
                mix = []
                for branch in range(2):
                    at = branch * groups * per_group + h
                    mix.append(jnp.where(low, gates[:, at : at + 1], gates[:, at + 1 : at + 2]))
                mixed = mix[0] * comp_out[part] + mix[1] * chosen_out[part]
                column = (g * pairs + p) * LANES
                out_ref[here, column : column + LANES] = mixed.astype(jnp.bfloat16)
        return 0

    lax.fori_loop(0, blocks, one_block, 0)


def attend(shape, span, picks, queries, gates, pairs, comp):
    blocks, groups, per_group, _ = shape
    rows = per_group // 2 * BLK
    smem = pl.BlockSpec(memory_space=pltpu.SMEM)
    vmem = pl.BlockSpec(memory_space=pltpu.VMEM)
    return pl.pallas_call(
        functools.partial(attend_kernel, shape),
        out_shape=jax.ShapeDtypeStruct(queries.shape, jnp.bfloat16),
        in_specs=[smem, smem, vmem, vmem, vmem, vmem],
        out_specs=vmem,
        scratch_shapes=[
            pltpu.VMEM((PICKS // 2, rows, 2 * LANES), jnp.float32),
            pltpu.SMEM((PICKS + 2,), jnp.int32),
        ],
        cost_estimate=pl.CostEstimate(
            flops=int(1e10), bytes_accessed=int(4e6), transcendentals=int(1e6)
        ),
    )(span, picks, queries, gates, pairs, comp)


def body(
    tokens, seq_lengths, block_picks, w_query, w_key, w_value, w_gate, w_ckey, w_cvalue, w_out
):
    token_rows = tokens[0]
    tok_count = token_rows.shape[0]
    width = token_rows.shape[1]
    spans = lax.axis_size("kv")
    copies = lax.axis_size("dp")
    shard_index = lax.axis_index("kv")
    head_index = lax.axis_index("tp")
    group_count = w_key.shape[1] // HEAD
    head_count = w_query.shape[1] // HEAD
    per_group = head_count // group_count
    block_count = tok_count // BLK

    def share(w):
        part = w.shape[0] // copies
        return lax.dynamic_slice_in_dim(w, lax.axis_index("dp") * part, part, 0)

    def gather_rows(w):
        return lax.all_gather(share(w), ("kv", "dp"), axis=0, tiled=True)

    kv_weight = gather_rows(jnp.concatenate([w_key, w_value], axis=1))
    query_weight = gather_rows(w_query)

    kv = jnp.dot(token_rows, kv_weight, preferred_element_type=jnp.float32).astype(jnp.bfloat16)
    split = kv.reshape(block_count, BLK, 2, group_count, HEAD)

    def compress(which, w):
        flat = split[:, :, which].transpose(0, 2, 1, 3).reshape(-1, BLK * HEAD)
        out = jnp.dot(flat, w, preferred_element_type=jnp.float32).astype(jnp.bfloat16)
        return out.reshape(block_count, group_count * HEAD)

    comp = jnp.concatenate([compress(0, w_ckey), compress(1, w_cvalue)], axis=1)
    pad = -block_count % 16
    packed = jnp.concatenate([kv, jnp.pad(comp, ((0, pad), (0, 0)))], axis=0)
    every = lax.all_gather(packed, "kv", axis=0)
    comp_all = every[:, tok_count : tok_count + block_count].reshape(spans * block_count, -1)
    comp_all = jnp.pad(comp_all, ((0, -comp_all.shape[0] % LANES), (0, 0)))

    queries = jnp.dot(token_rows, query_weight, preferred_element_type=jnp.float32)
    queries = queries.astype(jnp.bfloat16)
    gate_all = jax.nn.sigmoid(jnp.dot(token_rows, w_gate, preferred_element_type=jnp.float32))
    gates = lax.dynamic_slice_in_dim(
        gate_all.reshape(tok_count, 2, HEADS), head_index * head_count, head_count, 2
    ).reshape(tok_count, 2 * head_count)

    shape = (block_count, group_count, per_group, tok_count)
    attended = attend(
        shape,
        jnp.full((1,), shard_index, jnp.int32),
        block_picks[0].reshape(block_count, group_count * PICKS),
        queries,
        gates,
        every,
        comp_all,
    )

    out_parts = lax.all_gather(share(w_out), ("kv", "dp"), axis=0)
    out_parts = out_parts.reshape(spans, w_out.shape[0], w_out.shape[1])
    sides = lax.axis_size("tp")
    half_rows = tok_count // sides

    def project(side):
        rows = lax.dynamic_slice_in_dim(attended, side * half_rows, half_rows, 0)
        return [
            jnp.dot(rows, out_parts[i], preferred_element_type=jnp.float32).astype(jnp.bfloat16)
            for i in range(spans)
        ]

    swap = [(i, 1 - i) for i in range(sides)]
    theirs = jnp.concatenate(project(1 - head_index), axis=1)
    came = lax.ppermute(theirs, "tp", swap)
    mine = jnp.concatenate(project(head_index), axis=1)
    summed = mine.astype(jnp.float32) + came.astype(jnp.float32)
    out_positions = (
        shard_index * tok_count + head_index * half_rows + jnp.arange(half_rows, dtype=jnp.int32)
    )
    live_rows = out_positions < seq_lengths[0]
    return jnp.where(live_rows[:, None], summed, 0.0).astype(jnp.bfloat16)[None]


def solution(mesh):
    return jax.shard_map(
        body,
        mesh=mesh,
        in_specs=(
            P("dp", "kv", None),
            P("dp"),
            P("dp", "kv", "tp", None),
            P("kv", "tp"),
            P("kv", "tp"),
            P("kv", "tp"),
            P(),
            P(),
            P(),
            P("tp", "kv"),
        ),
        out_specs=P("dp", ("kv", "tp"), None),
        check_vma=False,
    )
```

time: 190 us -> 208 us (1.095)
  waiting for transfers between devices: 8.37 us -> 136 us
  blocking collectives: 83.2 us -> 20.3 us
  matrix products: 42 us -> 12.8 us
  local copies, waits for them, and re-layouts: 28.9 us -> 7.74 us
  Pallas kernels: 0 us -> 13.8 us
  other arithmetic: 7.92 us -> 2.78 us
  loops' own time: 4.76 us -> 0 us
    all_gather x2 -> x3, waiting for transfers between devices: 0.02 us -> 135 us  [the longest x2 90 us: gather_rows(): return lax.all_gather(share(w), ('kv', 'dp'), axis=0, tiled=True)]
    all_gather x4 -> x1, blocking collectives: 83.2 us -> 20.3 us  [body(): every = lax.all_gather(packed, 'kv', axis=0)]
    dot_general x42 -> x12, matrix products: 41.4 us -> 11.4 us  [the longest x8 5.59 us: project(): jnp.dot(rows, out_parts[i], preferred_element_type=jnp.float32)]
    pallas_call x0 -> x1, Pallas kernels: none -> 13.8 us  [attend(): pl.pallas_call(functools.partial(attend_kernel, shape), out_shape=jax.Sha...]
    dynamic_slice x25 -> x2, local copies, waits for them, and re-layouts: 10.8 us -> 3.15 us  [share(): return lax.dynamic_slice_in_dim(w, lax.axis_index('dp') * part, part, 0)]
    reduce_scatter x1 -> x0, waiting for transfers between devices: 6.93 us -> none  [body(): lax.psum_scatter(jnp.dot(attended, out_full, preferred_element_type=jnp.f...]
    while x12 -> x0, local copies, waits for them, and re-layouts: 6.29 us -> none
    another operation x1 -> x0, loops' own time: 4.76 us -> none  [body(): lax.map(attend, (queries, gate_local, pair_blocks, fetched, usable, jnp.a...]
  transfers between devices with their start and end apart: 3 -> 4, of which waited for: 1 -> 4; matrix products, arithmetic and copies ran while one was open for 35% -> 8% of each run, Pallas kernels for 0% -> 7%
where the time goes in v1:
time: 208 us
  waiting for transfers between devices  136 us (65%)
  blocking collectives  20.3 us (10%)
  between operations  14 us (7%)
  Pallas kernels  13.8 us (7%)
  matrix products  12.8 us (6%)
  local copies, waits for them, and re-layouts  7.74 us (4%)
  other arithmetic  2.78 us (1%)
    all_gather x2, waiting for transfers between devices, gather_rows(): return lax.all_gather(share(w), ('kv', 'dp'), axis=0, tiled=True)  90 us
    all_gather x1, waiting for transfers between devices, body(): out_parts = lax.all_gather(share(w_out), ('kv', 'dp'), axis=0)  45 us
    all_gather x1, blocking collectives, body(): every = lax.all_gather(packed, 'kv', axis=0)  20.3 us
    pallas_call x1, Pallas kernels, attend(): pl.pallas_call(functools.partial(attend_kernel, shape), out_shape=jax.Sha...  13.8 us
    dot_general x8, matrix products, project(): jnp.dot(rows, out_parts[i], preferred_element_type=jnp.float32)  5.59 us
  transfers between devices with their start and end apart: 4, of which 4 were waited for; matrix products, arithmetic and copies ran while one was open for 8% of the time, Pallas kernels for 7%

profile of v1, /device:TPU:0, one launch (start us, length us, event | category | flops | bytes accessed | tf_op | source)
XLA Modules:
  0.0 207.8 jit_solution(14405415000813417306)
XLA Ops:
  6.5 0.0 copy-start
  6.5 0.0 all-gather.8.cloned.1.call-start
  6.5 1.5 fusion.49
  8.1 0.0 all-gather.8.cloned.1.call-update
  8.1 0.0 all-gather.6.cloned.1.call-start
  8.1 1.6 constant_dynamic-slice_fusion.1
  9.7 0.0 all-gather.6.cloned.1.call-update
  9.7 0.0 all-gather.10.cloned.1.call-start
  9.8 1.6 constant_dynamic-slice_fusion
  11.4 0.0 all-gather.10.cloned.1.call-update
  12.1 1.4 reshape_squeeze.3.picks_ref
  13.4 0.0 copy-done
  13.4 1.5 fusion.27
  14.9 0.8 copy.28.gate_ref
  15.8 52.2 %all-gather.8.cloned.1.call-done = bf16[2048,256]{1,0:T(8,128)(2,1)} async-done(((bf16[128,256]{1,0:T(8,128)(2,1)}), bf16[2048,256]{1,0:T(8,128)(2,1)}) %all-gather.8.cloned.1.call-update) | async-done | bytes 1048592 | tf_op jit(solution)/shard_map/all_gather | solution.py:226
  67.9 2.0 fusion.15
  69.9 0.0 copy-start.2
  69.9 0.1 copy.23
  70.1 0.2 reshape.40
  70.3 0.0 copy-start.3
  70.3 0.3 slice_bitcast_fusion.1
  70.7 0.2 reshape.41
  70.9 0.1 copy-done.2
  71.0 0.2 convolution_convert_fusion.9
  71.2 0.1 reshape.42
  71.3 0.2 reshape.43
  71.5 0.2 convolution_convert_fusion.8
  71.8 0.1 reshape.44
  71.9 0.2 copy.26
  72.1 0.1 copy.27
  72.2 20.3 %all-gather = bf16[1600,256]{1,0:T(8,128)(2,1)S(1)} all-gather(bf16[400,256]{1,0:T(8,128)(2,1)S(1)} %copy.27), channel_id=2, replica_groups=mesh['dp'=4,'kv'=4,'tp'=2] {'kv'}, dimensions={0}, use_global_device_ids=true | all-gather | bytes 1024000 | tf_op jit(solution)/shard_map/all_gather | solution.py:242
  92.5 0.7 pad.9.comp_ref
  93.2 37.8 %all-gather.6.cloned.1.call-done = bf16[2048,512]{1,0:T(8,128)(2,1)} async-done(((bf16[128,512]{1,0:T(8,128)(2,1)}), bf16[2048,512]{1,0:T(8,128)(2,1)}) %all-gather.6.cloned.1.call-update) | async-done | bytes 2097168 | tf_op jit(solution)/shard_map/all_gather | solution.py:226
  131.0 3.3 %fusion.9.q_ref = bf16[384,512]{1,0:T(8,128)(2,1)} fusion(bf16[2048,512]{1,0:T(8,128)(2,1)} %all-gather.6.cloned.1.call-done, bf16[1,384,2048]{2,1,0:T(8,128)(2,1)S(1)} %copy-done), kind=kOutput, calls=%fused_computation.8 | convolution fusion | flops 805502976 | bytes 4063232 | tf_op jit(solution)/shard_map/dot_general | solution.py:246
  134.3 13.8 %shard_map.100 = bf16[384,512]{1,0:T(8,128)(2,1)} custom-call(s32[1]{0:T(128)} %bitcast.1.start_ref, s32[6,32]{1,0:T(8,128)} %reshape_squeeze.3.picks_ref, bf16[384,512]{1,0:T(8,128)(2,1)} %fusion.9.q_ref, f32[384,16]{1,0:T(8,128)} %copy.28.gate_ref, bf16[4,400,256]{2,1,0:T(8,128)(2,1)} %bitcast.56, bf16[128,256]{1,0:T(8,128)(2,1)} %pad.9.comp_ref), custom_call_target="tpu_custom_call" | custom-call | flops 10000000000 | bytes 4000000 | tf_op jit(solution)/shard_map/pallas_call | solution.py:191
  148.2 45.0 %all-gather.10.cloned.1.call-done = bf16[2048,512]{1,0:T(8,128)(2,1)} async-done(((bf16[128,512]{1,0:T(8,128)(2,1)}), bf16[2048,512]{1,0:T(8,128)(2,1)}) %all-gather.10.cloned.1.call-update) | async-done | bytes 2097168 | tf_op jit(solution)/shard_map/all_gather | solution.py:264
  193.2 1.5 convolution_convert_fusion.2
  194.7 1.4 convolution_convert_fusion.1
  196.1 1.3 convolution_convert_fusion
  197.5 0.3 convolution_convert_fusion.3
  197.7 0.1 pad_maximum_fusion
  197.8 0.1 collective-permute-start
  197.9 0.3 convolution_convert_fusion.6
  198.2 0.3 convolution_convert_fusion.5
  198.5 0.3 convolution_convert_fusion.4
  198.7 0.3 convolution_convert_fusion.7
  199.0 1.2 collective-permute-done
  200.2 1.1 fusion.30
  (15 shorter events, 0.2 us)
Async XLA Ops:
  6.5 6.9 %copy-start = (bf16[1,384,2048]{2,1,0:T(8,128)(2,1)S(1)}, bf16[1,384,2048]{2,1,0:T(8,128)(2,1)}, u32[]{:S(2)}) copy-start(bf16[1,384,2048]{2,1,0:T(8,128)(2,1)} %param.10) | copy-start | bytes 4718596
  6.5 61.4 %all-gather.8.cloned.1.call-start = ((), (), s32[]{:S(2)}) async-start(), calls=%async_computation.1 | async-start | bytes 1114112 | tf_op jit(solution)/shard_map/all_gather | solution.py:226
  8.1 122.9 %all-gather.6.cloned.1.call-start = ((), (), s32[]{:S(2)}) async-start(), calls=%async_computation | async-start | bytes 2228224 | tf_op jit(solution)/shard_map/all_gather | solution.py:226
  9.7 183.4 %all-gather.10.cloned.1.call-start = ((), (), s32[]{:S(2)}) async-start(), calls=%async_computation.2 | async-start | bytes 2228224 | tf_op jit(solution)/shard_map/all_gather | solution.py:264
  69.9 1.0 copy-start.2
  70.3 1.2 copy-start.3
  92.5 41.8 %copy-start.1 = (bf16[1600,256]{1,0:T(8,128)(2,1)}, bf16[1600,256]{1,0:T(8,128)(2,1)S(1)}, u32[]{:S(2)}) copy-start(bf16[1600,256]{1,0:T(8,128)(2,1)S(1)} %all-gather) | copy-start | bytes 2457604
  148.2 48.0 %copy-start.5 = (bf16[384,512]{1,0:T(8,128)(2,1)S(1)}, bf16[384,512]{1,0:T(8,128)(2,1)}, u32[]{:S(2)}) copy-start(bf16[384,512]{1,0:T(8,128)(2,1)} %shard_map.100) | copy-start | bytes 1179652
  193.1 4.3 %copy-start.4 = (bf16[2048,512]{1,0:T(8,128)(2,1)S(1)}, bf16[2048,512]{1,0:T(8,128)(2,1)}, u32[]{:S(2)}) copy-start(bf16[2048,512]{1,0:T(8,128)(2,1)} %all-gather.10.cloned.1.call-done) | copy-start | bytes 6291460
  197.8 2.4 %collective-permute-start = (bf16[192,2048]{1,0:T(8,128)(2,1)S(1)}, bf16[192,2048]{1,0:T(8,128)(2,1)S(1)}, u32[]{:S(2)}, u32[]{:S(2)}) collective-permute-start(bf16[192,2048]{1,0:T(8,128)(2,1)S(1)} %pad_maximum_fusion), channel_id=1, source_target_pairs={{0,1},{1,0},{2,3},{3,2},{4,5},{5,4},{6,7},{7,6},{8,9},{9,8},{10,11... | collective-permute-start | bytes 2359304 | tf_op jit(solution)/shard_map/ppermute | solution.py:278
Sparse Core Ops, SparseCore 0:
  10.1 57.7 all-gather.7
  70.7 60.2 all-gather.5
  133.8 59.3 all-gather.9
